TPU v7x, 32 devices: a whole 2x2x4 slice. The times are simulated.
32 devices in a mesh: ep: 8 (over z, x), tp: 4 (over y, core).
Axes of the slice: x: 2, y: 2, z: 4, core: 2. Of those that a mesh axis runs over, the one named last changes fastest.
Arguments:
- queries: bfloat16 [4096, 1024], P('ep', 'tp'), may hold values from -6 to 6
- key_input: bfloat16 [4096, 256], P('ep'), may hold values from -6 to 6
- value_input: bfloat16 [4096, 256], P('ep'), may hold values from -6 to 6
- query_gain: float32 [64], replicated, may hold values from 0.1 to 1.9
- key_gain: float32 [64], replicated, may hold values from 0.1 to 1.9
- mix_out_weight: bfloat16 [1024, 2048], P('tp'), may hold values from -0.1875 to 0.1875
- expert_input: bfloat16 [1280, 2048], P('ep'), may hold values from -6 to 6
- ffn_gain: float32 [2048], replicated, may hold values from 0.1 to 1.9
- routes: int32 [1280, 2], P('ep'), may hold values from 0 to 7, all different within a row; in each aligned block of 160 rows (0 to 159, 160 to 319, ...) at most 60 rows name the same one
- route_scores: float32 [1280, 2], P('ep'), may hold values from 0.1 to 1
- gate_weight: bfloat16 [8, 2048, 4096], P('ep', None, 'tp'), may hold values from -0.125 to 0.125
- up_weight: bfloat16 [8, 2048, 4096], P('ep', None, 'tp'), may hold values from -0.125 to 0.125
- down_weight: bfloat16 [8, 4096, 2048], P('ep', 'tp'), may hold values from -0.09375 to 0.09375
Outputs:
- mixed_rows: bfloat16 [4096, 2048], P(('ep', 'tp'))
- expert_out: bfloat16 [1280, 2048], P('ep', 'tp')
Inputs may be any that keep to these rules, and one draw needn't show every extreme that they name: `routes`: each row names 2 different experts. Within the rows of one index of ep (aligned blocks of 160 rows) no expert is named by more than 60 rows, and in every draw some expert is named by exactly 60 rows of some block.
All inputs are finite; a program needn't handle non-finite values.
Results may differ from a plain program's by a relative error of at most 0.019.
The roundings to bfloat16 on the way count: a program that leaves them out, or rounds other values in their place, can miss the bound.
Values may be sent and summed in bfloat16 or wider, within the bound.
A program may use at most 64 MiB of HBM per device.

v0:
```python
import math

import jax
import jax.numpy as jnp
from jax import lax
from jax.sharding import PartitionSpec as P

HEADS = 16
KV_HEADS = 4
HD = 64
GRID_W = 64


EPSILON = 1e-06
ROPE_BASE = 10000.0


def rotate_half(portion, cos_table, sin_table):
    front_half, back_half = jnp.split(portion, 2, axis=-1)
    cos_table = cos_table[:, None, :]
    sin_table = sin_table[:, None, :]
    return jnp.concatenate(
        [
            front_half * cos_table - back_half * sin_table,
            back_half * cos_table + front_half * sin_table,
        ],
        axis=-1,
    )


def prepare(source, channel_gain, positions):
    token_count = source.shape[0]
    values_f = source.astype(jnp.float32).reshape(token_count, -1, HD)
    normed = (
        values_f
        * lax.rsqrt(jnp.mean(values_f * values_f, axis=-1, keepdims=True) + EPSILON)
        * channel_gain
    )
    quarter = HD // 4
    inverse = ROPE_BASE ** (-jnp.arange(quarter, dtype=jnp.float32) / quarter)
    row_angle = (positions // GRID_W).astype(jnp.float32)[:, None] * inverse[None, :]
    col_angle = (positions % GRID_W).astype(jnp.float32)[:, None] * inverse[None, :]
    half_width = HD // 2
    turned = jnp.concatenate(
        [
            rotate_half(normed[..., :half_width], jnp.cos(row_angle), jnp.sin(row_angle)),
            rotate_half(normed[..., half_width:], jnp.cos(col_angle), jnp.sin(col_angle)),
        ],
        axis=-1,
    )
    return turned.reshape(token_count, -1).astype(jnp.bfloat16)


def local(
    queries,
    key_input,
    value_input,
    query_gain,
    key_gain,
    mix_out_weight,
    expert_input,
    ffn_gain,
    routes,
    route_scores,
    gate_weight,
    up_weight,
    down_weight,
):
    row_count = queries.shape[0]
    heads_here = queries.shape[1] // HD
    group_size = HEADS // KV_HEADS
    kv_here = max(1, heads_here // group_size)
    sharing = heads_here // kv_here
    tp_count = lax.axis_size("tp")
    tp_index = lax.axis_index("tp")
    positions = lax.axis_index("ep") * row_count + jnp.arange(row_count, dtype=jnp.int32)
    first_kv = tp_index * heads_here // group_size
    own_keys = lax.dynamic_slice_in_dim(key_input, first_kv * HD, kv_here * HD, 1)
    own_values = lax.dynamic_slice_in_dim(value_input, first_kv * HD, kv_here * HD, 1)
    q_rot = prepare(queries, query_gain, positions).reshape(row_count, kv_here, sharing, HD)
    start_state = (
        jnp.zeros((row_count, kv_here, sharing, HD), jnp.float32),
        jnp.zeros((row_count, kv_here, sharing), jnp.float32),
    )
    running = start_state
    key_piece = lax.all_gather(own_keys, "ep", axis=0, tiled=True)
    value_piece = lax.all_gather(own_values, "ep", axis=0, tiled=True)
    key_count = key_piece.shape[0]
    key_piece = prepare(key_piece, key_gain, jnp.arange(key_count, dtype=jnp.int32))
    key_span = math.gcd(key_count, 1024)
    key_blocks = key_piece.reshape(key_count // key_span, key_span, kv_here, HD)
    value_blocks = value_piece.reshape(key_count // key_span, key_span, kv_here, HD)

    def one_block(partial_value, block_pair):
        key_block, value_block = block_pair
        scores = jnp.einsum(
            "qgrd,kgd->qgrk", q_rot, key_block, preferred_element_type=jnp.float32
        ) * HD ** (-0.5)
        weights = jnp.exp(scores)
        weighted = partial_value[0] + jnp.einsum(
            "qgrk,kgd->qgrd",
            weights.astype(jnp.bfloat16),
            value_block,
            preferred_element_type=jnp.float32,
        )
        return ((weighted, partial_value[1] + jnp.sum(weights, axis=-1)), None)

    running, _ = lax.scan(one_block, running, (key_blocks, value_blocks))
    weighted, denominator = running
    attended = (
        (weighted / denominator[..., None]).astype(jnp.bfloat16).reshape(row_count, heads_here * HD)
    )
    token_count = routes.shape[0]
    top_count = routes.shape[1]
    expert_count = lax.axis_size("ep")
    model_width = expert_input.shape[1]
    feat_width = model_width // tp_count
    capacity = 3 * token_count * top_count // (2 * expert_count)
    flat_routes = routes.reshape(-1)
    hit_table = (flat_routes[:, None] == jnp.arange(expert_count, dtype=jnp.int32)[None, :]).astype(
        jnp.int32
    )
    position = jnp.sum((jnp.cumsum(hit_table, axis=0) - hit_table) * hit_table, axis=1)
    slot_index = flat_routes * capacity + position
    pair_token = jnp.arange(token_count * top_count, dtype=jnp.int32) // top_count
    owner_row = (
        jnp.full((expert_count * capacity,), token_count, jnp.int32).at[slot_index].set(pair_token)
    )
    own_features = lax.dynamic_slice_in_dim(expert_input, tp_index * feat_width, feat_width, 1)
    padded = jnp.concatenate([own_features, jnp.zeros((1, feat_width), jnp.bfloat16)], axis=0)
    outbound = padded[owner_row]
    arrived = lax.all_to_all(outbound, "ep", split_axis=0, concat_axis=0, tiled=True)
    gate_local = gate_weight[0]
    up_local = up_weight[0]
    down_local = down_weight[0]
    values_f = lax.all_gather(arrived, "tp", axis=1, tiled=True).astype(jnp.float32)
    scaled = (values_f * ffn_gain).astype(jnp.bfloat16)
    gate_sum = jnp.dot(scaled, gate_local, preferred_element_type=jnp.float32)
    up_sum = jnp.dot(scaled, up_local, preferred_element_type=jnp.float32)
    squares = jnp.sum(values_f * values_f, axis=1)
    row_scale = lax.rsqrt(squares / model_width + EPSILON)[:, None]
    hidden = (jax.nn.silu(row_scale * gate_sum) * (row_scale * up_sum)).astype(jnp.bfloat16)
    mixed_sum = lax.psum_scatter(
        jnp.dot(attended, mix_out_weight, preferred_element_type=jnp.float32).astype(jnp.bfloat16),
        "tp",
        scatter_dimension=0,
        tiled=True,
    )
    width_sum = lax.psum_scatter(
        lax.dot_general(
            down_local, hidden, (((0,), (1,)), ((), ())), preferred_element_type=jnp.float32
        ).astype(jnp.bfloat16),
        "tp",
        scatter_dimension=0,
        tiled=True,
    )
    returned_rows = lax.all_to_all(width_sum, "ep", split_axis=1, concat_axis=1, tiled=True)
    route_weight = route_scores / jnp.sum(route_scores, axis=-1, keepdims=True)
    picked = returned_rows[:, slot_index].astype(jnp.float32) * route_weight.reshape(-1)[None, :]
    combined = jnp.sum(picked.reshape(feat_width, token_count, top_count), axis=-1)
    return (mixed_sum, combined.T.astype(jnp.bfloat16))


def solution(mesh):
    placed = (
        P("ep", "tp"),
        P("ep", None),
        P("ep", None),
        P(),
        P(),
        P("tp", None),
        P("ep", None),
        P(),
        P("ep", None),
        P("ep", None),
        P("ep", None, "tp"),
        P("ep", None, "tp"),
        P("ep", "tp", None),
    )
    return jax.shard_map(
        local,
        mesh=mesh,
        in_specs=placed,
        out_specs=(P(("ep", "tp"), None), P("ep", "tp")),
        check_vma=False,
    )
```

profile of v0, /device:TPU:8, one launch (start us, length us, event | category | flops | bytes accessed | tf_op | source)
XLA Modules:
  0.0 199.0 jit_solution(4162762366522930268)
XLA Ops:
  10.5 2.9 %scatter_custom_fusion = s32[480]{0:T(512)S(1)} fusion(s32[320]{0:T(512)S(1)} %fusion.85, s32[320]{0:T(512)S(1)} %add_select_fusion.1, s32[]{:T(128)} %constant.138.clone.1), kind=kCustom, calls=%fused_computation.132 | custom fusion | bytes 1924 | tf_op jit(solution)/shard_map/scatter | solution.py:127
  14.4 2.1 %gather_fusion = bf16[480,512]{1,0:T(8,128)(2,1)S(1)} fusion(bf16[161,512]{1,0:T(8,128)(2,1)S(1)} %concatenate.30, s32[1024]{0:T(1024)S(1)} %pad_clamp_fusion.1), kind=kCustom, calls=%fused_computation | custom fusion | bytes 984960 | tf_op jit(solution)/shard_map/gather | solution.py:131
  17.4 6.3 %all-to-all-start = ((bf16[8,60,512]{2,1,0:T(8,128)(2,1)}), bf16[8,60,512]{2,1,0:T(8,128)(2,1)S(1)}, u32[]{:S(2)}, u32[]{:S(2)}) async-start(bf16[8,60,512]{2,1,0:T(8,128)(2,1)} %all_to_all.16), calls=%async_computation.1 | async-start | bytes 1048576 | tf_op jit(solution)/shard_map/all_to_all | solution.py:132
  23.9 35.1 %all_gather.10 = bf16[4096,64]{0,1:T(8,128)(2,1)S(1)} all-gather(bf16[512,64]{0,1:T(8,128)(2,1)S(1)} %copy.39), channel_id=1, replica_groups=mesh['ep'=8,'tp'=4] {'ep'}, dimensions={0}, use_global_device_ids=true | all-gather | bytes 589824 | tf_op jit(solution)/shard_map/all_gather | solution.py:86
  60.4 2.3 %fusion.60 = (bf16[4096,1,16]{0,2,1:T(8,128)(2,1)S(1)}, bf16[4096,1,16]{0,2,1:T(8,128)(2,1)S(1)}, bf16[4096,1,16]{0,2,1:T(8,128)(2,1)S(1)}, bf16[4096,1,16]{0,2,1:T(8,128)(2,1)S(1)}) fusion(f32[4096,1,64]{0,2,1:T(8,128)S(1)} %fusion.44, f32[16]{0:T(128)S(1)} %multiply_power_fusion, f32[4096]{0:T(1024)S(1)} %get-tuple-element.102, f32[4096]{0:T(1024)S(1)} %get-tuple-element.103), kind=kLoop, calls=%fused_computation.65 | loop fusion | flops 1179648 | bytes 1605696 | tf_op jit(solution)/shard_map/convert.13
  63.6 33.2 %all_gather.9 = bf16[4096,64]{1,0:T(8,128)(2,1)S(1)} all-gather(bf16[512,64]{1,0:T(8,128)(2,1)S(1)} %constant_dynamic-slice_fusion.2), channel_id=1, replica_groups=mesh['ep'=8,'tp'=4] {'ep'}, dimensions={0}, use_global_device_ids=true | all-gather | bytes 589824 | tf_op jit(solution)/shard_map/all_gather | solution.py:87
  98.0 2.0 %fusion.24 = f32[480]{0:T(512)S(1)} fusion(bf16[480,2048]{1,0:T(8,128)(2,1)} %all-gather.2.cloned.1.call-done), kind=kLoop, calls=%fused_computation.28 | loop fusion | flops 2948640 | bytes 1968000 | tf_op jit(solution)/shard_map/reduce_sum | solution.py:140
  100.0 6.3 %fusion.20 = f32[480,1024]{1,0:T(8,128)} fusion(bf16[1,2048,1024]{2,1,0:T(8,128)(2,1)} %param.26, bf16[480,2048]{1,0:T(8,128)(2,1)} %all-gather.2.cloned.1.call-done, f32[2048]{0:T(1024)S(1)} %copy-done.7), kind=kOutput, calls=%fused_computation.24 | convolution fusion | flops 2016215040 | bytes 8134656 | tf_op jit(solution)/shard_map/dot_general | solution.py:139
  106.3 10.5 %fusion.29 = bf16[2048,480]{0,1:T(8,128)(2,1)} fusion(bf16[1,1024,2048]{2,1,0:T(8,128)(2,1)} %param.27, f32[480,1024]{1,0:T(8,128)} %fusion.20, bf16[1,2048,1024]{2,1,0:T(8,128)(2,1)} %param.25, bf16[480,2048]{1,0:T(8,128)(2,1)} %all-gather.2.cloned.1.call-done, f32[2048]{0:T(1024)S(1)} %copy-done.7, f32[480]{0:T(512)S(1)} %add_rsqrt_fusion.2), kind=kOutput, calls=%fused_computation.32 | convolution fusion | flops 4034396160 | bytes 14296960 | tf_op jit(solution)/shard_map/dot_general | solution.py:150
  117.0 42.0 %while.13 = (s32[]{:T(128)}, f32[512,1,4,64]{0,3,2,1:T(8,128)S(1)}, f32[512,1,4]{0,2,1:T(4,128)S(1)}, bf16[4,1024,1,64]{1,3,2,0:T(8,128)(2,1)S(1)}, bf16[4,1024,...) while((s32[]{:T(128)}, f32[512,1,4,64]{0,3,2,1:T(8,128)S(1)}, ...), condition=%wide.region_4.5_spmd.clone, body=%wide.region_2.4_spmd.clone.sunk | while | flops 545523712 | bytes 18383460 | solution.py:108
  117.1 5.4 %bitcast_reduce_fusion.2 = (f32[512,4]{0,1:T(4,128)S(1)}, f32[1024,512,4]{1,0,2:T(8,128)}) fusion(bf16[512,1,4,64]{0,3,2,1:T(8,128)(2,1)S(1)} %get-tuple-element.168, bf16[4,1024,1,64]{1,3,2,0:T(8,128)(2,1)} %get-tuple-element.167, s32[]{:T(128)} %get-tuple-element.155), kind=kOutput, calls=%fused_computation.3.clone.1 | convolution fusion | flops 272627712 | bytes 8790528 | tf_op jit(solution)/shard_map/while/body/eval_jaxpr/qgrd,kgd->qgrk/dot_general | solution.py:96
  122.5 5.4 %fusion.97 = f32[512,1,4,64]{0,3,2,1:T(8,128)S(1)} fusion(f32[1024,512,4]{1,0,2:T(8,128)} %get-tuple-element.145, f32[512,1,4,64]{0,3,2,1:T(8,128)S(1)} %get-tuple-element.156, pred[]{:T(512)S(6)} %compare.25, bf16[4,1024,1,64]{1,3,2,0:T(8,128)(2,1)S(1)} %get-tuple-element.166, s32[]{:T(128)} %get-tuple-element.155), kind=kOutput, calls=%fused_computation.9.clone.1 | convolution fusion | flops 272891904 | bytes 9568261 | tf_op jit(solution)/shard_map/while/body/eval_jaxpr/qgrk,kgd->qgrd/dot_general | solution.py:100
  128.0 5.4 %bitcast_reduce_fusion.2 = (f32[512,4]{0,1:T(4,128)S(1)}, f32[1024,512,4]{1,0,2:T(8,128)}) fusion(bf16[512,1,4,64]{0,3,2,1:T(8,128)(2,1)S(1)} %get-tuple-element.168, bf16[4,1024,1,64]{1,3,2,0:T(8,128)(2,1)} %get-tuple-element.167, s32[]{:T(128)} %get-tuple-element.155), kind=kOutput, calls=%fused_computation.3.clone.1 | convolution fusion | flops 272627712 | bytes 8790528 | tf_op jit(solution)/shard_map/while/body/eval_jaxpr/qgrd,kgd->qgrk/dot_general | solution.py:96
  133.4 5.0 %fusion.97 = f32[512,1,4,64]{0,3,2,1:T(8,128)S(1)} fusion(f32[1024,512,4]{1,0,2:T(8,128)} %get-tuple-element.145, f32[512,1,4,64]{0,3,2,1:T(8,128)S(1)} %get-tuple-element.156, pred[]{:T(512)S(6)} %compare.25, bf16[4,1024,1,64]{1,3,2,0:T(8,128)(2,1)S(1)} %get-tuple-element.166, s32[]{:T(128)} %get-tuple-element.155), kind=kOutput, calls=%fused_computation.9.clone.1 | convolution fusion | flops 272891904 | bytes 9568261 | tf_op jit(solution)/shard_map/while/body/eval_jaxpr/qgrk,kgd->qgrd/dot_general | solution.py:100
  138.4 5.4 %bitcast_reduce_fusion.2 = (f32[512,4]{0,1:T(4,128)S(1)}, f32[1024,512,4]{1,0,2:T(8,128)}) fusion(bf16[512,1,4,64]{0,3,2,1:T(8,128)(2,1)S(1)} %get-tuple-element.168, bf16[4,1024,1,64]{1,3,2,0:T(8,128)(2,1)} %get-tuple-element.167, s32[]{:T(128)} %get-tuple-element.155), kind=kOutput, calls=%fused_computation.3.clone.1 | convolution fusion | flops 272627712 | bytes 8790528 | tf_op jit(solution)/shard_map/while/body/eval_jaxpr/qgrd,kgd->qgrk/dot_general | solution.py:96
  143.8 4.9 %fusion.97 = f32[512,1,4,64]{0,3,2,1:T(8,128)S(1)} fusion(f32[1024,512,4]{1,0,2:T(8,128)} %get-tuple-element.145, f32[512,1,4,64]{0,3,2,1:T(8,128)S(1)} %get-tuple-element.156, pred[]{:T(512)S(6)} %compare.25, bf16[4,1024,1,64]{1,3,2,0:T(8,128)(2,1)S(1)} %get-tuple-element.166, s32[]{:T(128)} %get-tuple-element.155), kind=kOutput, calls=%fused_computation.9.clone.1 | convolution fusion | flops 272891904 | bytes 9568261 | tf_op jit(solution)/shard_map/while/body/eval_jaxpr/qgrk,kgd->qgrd/dot_general | solution.py:100
  148.7 5.4 %bitcast_reduce_fusion.2 = (f32[512,4]{0,1:T(4,128)S(1)}, f32[1024,512,4]{1,0,2:T(8,128)}) fusion(bf16[512,1,4,64]{0,3,2,1:T(8,128)(2,1)S(1)} %get-tuple-element.168, bf16[4,1024,1,64]{1,3,2,0:T(8,128)(2,1)} %get-tuple-element.167, s32[]{:T(128)} %get-tuple-element.155), kind=kOutput, calls=%fused_computation.3.clone.1 | convolution fusion | flops 272627712 | bytes 8790528 | tf_op jit(solution)/shard_map/while/body/eval_jaxpr/qgrd,kgd->qgrk/dot_general | solution.py:96
  154.1 4.9 %fusion.97 = f32[512,1,4,64]{0,3,2,1:T(8,128)S(1)} fusion(f32[1024,512,4]{1,0,2:T(8,128)} %get-tuple-element.145, f32[512,1,4,64]{0,3,2,1:T(8,128)S(1)} %get-tuple-element.156, pred[]{:T(512)S(6)} %compare.25, bf16[4,1024,1,64]{1,3,2,0:T(8,128)(2,1)S(1)} %get-tuple-element.166, s32[]{:T(128)} %get-tuple-element.155), kind=kOutput, calls=%fused_computation.9.clone.1 | convolution fusion | flops 272891904 | bytes 9568261 | tf_op jit(solution)/shard_map/while/body/eval_jaxpr/qgrk,kgd->qgrd/dot_general | solution.py:100
  159.1 2.1 %convolution_convert_fusion = bf16[512,2048]{1,0:T(8,128)(2,1)} fusion(bf16[512,256]{0,1:T(8,128)(2,1)S(1)} %bitcast.122, bf16[256,2048]{1,0:T(8,128)(2,1)S(1)} %copy-done), kind=kOutput, calls=%fused_computation.30 | convolution fusion | flops 537919488 | bytes 3407872 | tf_op jit(solution)/shard_map/dot_general | solution.py:144
  161.3 1.9 all_to_all.19
  163.2 6.0 %all-to-all-start.1 = ((bf16[512,8,60]{0,2,1:T(8,128)(2,1)}), bf16[512,8,60]{0,2,1:T(8,128)(2,1)S(1)}, u32[]{:S(2)}, u32[]{:S(2)}) async-start(bf16[512,8,60]{0,2,1:T(8,128)(2,1)} %all_to_all.19), calls=%async_computation.3 | async-start | bytes 1048576 | tf_op jit(solution)/shard_map/all_to_all | solution.py:157
  169.3 8.3 %all-to-all-done.1 = bf16[512,8,60]{0,2,1:T(8,128)(2,1)S(1)} async-done(((bf16[512,8,60]{0,2,1:T(8,128)(2,1)}), bf16[512,8,60]{0,2,1:T(8,128)(2,1)S(1)}, u32[]{:S(2)}, u32[]{:S(2)}) %all-to-all-start.1) | async-done | bytes 491552 | tf_op jit(solution)/shard_map/all_to_all | solution.py:157
  177.7 2.0 %gather_fusion.1 = bf16[320,512]{1,0:T(8,128)(2,1)S(1)} fusion(bf16[512,480]{0,1:T(8,128)(2,1)S(1)} %all_to_all.21, s32[1024]{0:T(1024)S(1)} %pad_clamp_fusion), kind=kCustom, calls=%fused_computation.1 | custom fusion | bytes 656640 | tf_op jit(solution)/shard_map/gather | solution.py:159
  181.8 10.7 %reduce-scatter.3.cloned.1.call-done = bf16[128,2048]{1,0:T(8,128)(2,1)} async-done(((bf16[512,2048]{1,0:T(8,128)(2,1)}), bf16[128,2048]{1,0:T(8,128)(2,1)}) %reduce-scatter.3.cloned.1.call-update) | async-done | bytes 524304 | tf_op jit(solution)/shard_map/reduce_scatter | solution.py:143
  (80 shorter events, 11.3 us)
Async XLA Ops:
  7.2 151.9 %copy-start = (bf16[256,2048]{1,0:T(8,128)(2,1)S(1)}, bf16[256,2048]{1,0:T(8,128)(2,1)}, u32[]{:S(2)}) copy-start(bf16[256,2048]{1,0:T(8,128)(2,1)} %param.20) | copy-start | bytes 3145732
  7.2 16.5 %copy-start.2 = (bf16[512,256]{1,0:T(8,128)(2,1)S(1)}, bf16[512,256]{1,0:T(8,128)(2,1)}, u32[]{:S(2)}) copy-start(bf16[512,256]{1,0:T(8,128)(2,1)} %param.16) | copy-start | bytes 786436
  14.4 44.8 %copy-start.5 = (f32[64]{0:T(128)S(1)}, f32[64]{0:T(128)}, u32[]{:S(2)}) copy-start(f32[64]{0:T(128)} %param.19) | copy-start | bytes 772
  17.4 42.0 %all-to-all-start = ((bf16[8,60,512]{2,1,0:T(8,128)(2,1)}), bf16[8,60,512]{2,1,0:T(8,128)(2,1)S(1)}, u32[]{:S(2)}, u32[]{:S(2)}) async-start(bf16[8,60,512]{2,1,0:T(8,128)(2,1)} %all_to_all.16), calls=%async_computation.1 | async-start | bytes 1048576 | tf_op jit(solution)/shard_map/all_to_all | solution.py:132
  23.6 74.4 %all-gather.2.cloned.1.call-start = ((), (), s32[]{:S(2)}) async-start(), calls=%async_computation.5 | async-start | bytes 2457600 | tf_op jit(solution)/shard_map/all_gather | solution.py:136
  59.4 37.8 %copy-start.1 = (bf16[512,256]{1,0:T(8,128)(2,1)S(1)}, bf16[512,256]{1,0:T(8,128)(2,1)}, u32[]{:S(2)}) copy-start(bf16[512,256]{1,0:T(8,128)(2,1)} %param.15) | copy-start | bytes 786436
  60.3 3.2 %copy-start.3 = (bf16[512,256]{1,0:T(8,128)(2,1)S(1)}, bf16[512,256]{1,0:T(8,128)(2,1)}, u32[]{:S(2)}) copy-start(bf16[512,256]{1,0:T(8,128)(2,1)} %param.17) | copy-start | bytes 786436
  60.3 100.9 %reduce-scatter.5.cloned.1.call-start = ((), (), s32[]{:S(2)}) async-start(), calls=%async_computation.6 | async-start | bytes 2457600 | tf_op jit(solution)/shard_map/reduce_scatter | solution.py:149
  60.4 37.4 %copy-start.6 = (f32[64]{0:T(128)S(1)}, f32[64]{0:T(128)}, u32[]{:S(2)}) copy-start(f32[64]{0:T(128)} %param.18) | copy-start | bytes 772
  96.8 3.2 %copy-start.7 = (f32[2048]{0:T(1024)S(1)}, f32[2048]{0:T(1024)}, u32[]{:S(2)}) copy-start(f32[2048]{0:T(1024)} %param.22) | copy-start | bytes 24580
  116.8 75.6 %reduce-scatter.3.cloned.1.call-start = ((), (), s32[]{:S(2)}) async-start(), calls=%async_computation.4 | async-start | bytes 2621440 | tf_op jit(solution)/shard_map/reduce_scatter | solution.py:143
  159.1 10.1 %copy-start.4 = (f32[160,2]{0,1:T(2,128)S(1)}, f32[160,2]{0,1:T(2,128)}, u32[]{:S(2)}) copy-start(f32[160,2]{0,1:T(2,128)} %param.24) | copy-start | bytes 3844
  163.2 14.4 %all-to-all-start.1 = ((bf16[512,8,60]{0,2,1:T(8,128)(2,1)}), bf16[512,8,60]{0,2,1:T(8,128)(2,1)S(1)}, u32[]{:S(2)}, u32[]{:S(2)}) async-start(bf16[512,8,60]{0,2,1:T(8,128)(2,1)} %all_to_all.19), calls=%async_computation.3 | async-start | bytes 1048576 | tf_op jit(solution)/shard_map/all_to_all | solution.py:157
Sparse Core Ops, SparseCore 0:
  60.4 21.8 all-gather.1
  116.9 30.1 reduce-scatter.4
  161.4 31.0 reduce-scatter.2
where the time goes:
time: 201 us; the launch traced here: 199 us
  blocking collectives  68.3 us (34%)
  matrix products  60.7 us (30%)
  waiting for transfers between devices  19 us (9%)
  local copies, waits for them, and re-layouts  15.4 us (8%)
  between operations  14.2 us (7%)
  starting transfers between devices  12.5 us (6%)
  other arithmetic  8.75 us (4%)
    all_gather x1, blocking collectives, local(): key_piece = lax.all_gather(own_keys, 'ep', axis=0, tiled=True)  35.1 us
    all_gather x1, blocking collectives, local(): value_piece = lax.all_gather(own_values, 'ep', axis=0, tiled=True)  33.2 us
    dot_general x4, matrix products, one_block(): jnp.einsum('qgrd,kgd->qgrk', q_rot, key_block, preferred_element_type=jnp...  21.6 us
    dot_general x4, matrix products, one_block(): jnp.einsum('qgrk,kgd->qgrd', weights.astype(jnp.bfloat16), value_block, p...  20.2 us
    reduce_scatter x1, waiting for transfers between devices, local(): lax.psum_scatter(jnp.dot(attended, mix_out_weight, preferred_element_type...  10.7 us
    dot_general x1, matrix products, local(): lax.dot_general(down_local, hidden, (((0,), (1,)), ((), ())), preferred_e...  10.5 us
    all_to_all x1, waiting for transfers between devices, local(): lax.all_to_all(width_sum, 'ep', split_axis=1, concat_axis=1, tiled=True)  8.28 us
    dot_general x1, matrix products, local(): up_sum = jnp.dot(scaled, up_local, preferred_element_type=jnp.float32)  6.26 us
  transfers between devices with their start and end apart: 5, of which 2 were waited for; matrix products, arithmetic and copies ran while one was open for 27% of the time, Pallas kernels for 0%

commit v1 on v0

v1 whole, which is shorter than its diff:
```python
import functools
import math

import jax
import jax.numpy as jnp
from jax import lax
from jax.experimental import pallas as pl
from jax.experimental.pallas import tpu as pltpu
from jax.sharding import PartitionSpec as P

HEADS = 16
KV_HEADS = 4
HD = 64
GRID_W = 64
EPSILON = 1e-06
ROPE_BASE = 10000.0
MESH = pl.DeviceIdType.MESH
LANES = 128
BF = jnp.bfloat16
F32 = jnp.float32


def prep(values, gain, cos_table, sin_table):
    width = values.shape[1]
    squares = values * values
    high = squares.astype(BF)
    low = (squares - high.astype(F32)).astype(BF)
    rows = lax.broadcasted_iota(jnp.int32, (width, width), 0) // HD
    cols = lax.broadcasted_iota(jnp.int32, (width, width), 1) // HD
    same = jnp.where(rows == cols, 1.0, 0.0).astype(BF)
    total = jnp.dot(high, same, preferred_element_type=F32) + jnp.dot(
        low, same, preferred_element_type=F32
    )
    normed = values * lax.rsqrt(total * (1.0 / HD) + EPSILON) * gain
    lane = lax.broadcasted_iota(jnp.int32, normed.shape, 1)
    quarter = HD // 4
    partner = jnp.where(
        lane % (2 * quarter) < quarter,
        pltpu.roll(normed, width - quarter, 1),
        pltpu.roll(normed, quarter, 1),
    )
    return normed * cos_table + partner * sin_table


def kernel(
    n_ep, n_tp, heads, model_width,
    q_ref, kv_ref, qg_ref, kg_ref, cos_ref, sin_ref, wmix_ref, x_ref, gain_ref, routes_ref,
    scores_ref, wg_ref, wu_ref, wd_ref,
    mixed_ref, out_ref,
    kv_buf, q_buf, x_out, x_buf, scaled, hid, wg, wu, wd, wmix, dp_buf, ep_in, es_buf, ey_in,
    ret_out, ret_in, mp_out, mp_in, ms_out, my_in, own_mix,
    w_sem, kv_s, kv_r, di_s, di_r, dy_s, dy_r, dc_s, dc_r, ep_s, ep_r, ey_s, ey_r, rt_s, rt_r,
    mp_s, mp_r, my_s, my_r,
):
    n_y = n_tp // 2
    me = lax.axis_index("ep")
    tp = lax.axis_index("tp")
    my_y, core = tp // 2, tp % 2
    mate = my_y * 2 + 1 - core
    rows = kv_ref.shape[0]
    slots_per = x_buf.shape[2]
    slots = n_ep * slots_per
    col_w = x_buf.shape[3]
    tokens = x_ref.shape[0]

    def y_peer(j):
        return (my_y + j) % n_y

    loads = [
        pltpu.make_async_copy(src, dst, w_sem.at[i])
        for i, (src, dst) in enumerate(
            ((wg_ref.at[0], wg), (wu_ref.at[0], wu), (wd_ref.at[0], wd), (wmix_ref, wmix))
        )
    ]
    for load in loads:
        load.start()

    barrier = pltpu.get_barrier_semaphore()

    def greet(o, carry):
        pl.semaphore_signal(barrier, inc=1, device_id=((me + o) % n_ep, tp), device_id_type=MESH)
        return carry

    lax.fori_loop(1, n_ep, greet, 0)
    for j in range(1, n_y):
        pl.semaphore_signal(
            barrier, inc=1, device_id=(me, y_peer(j) * 2 + core), device_id_type=MESH
        )
    pl.semaphore_signal(barrier, inc=1, device_id=(me, mate), device_id_type=MESH)

    expert_row = lax.broadcasted_iota(jnp.int32, (n_ep, tokens), 0)
    first = jnp.where(expert_row == routes_ref[0:1, :], 1.0, 0.0)
    second = jnp.where(expert_row == routes_ref[1:2, :], 1.0, 0.0)
    earlier = jnp.where(
        lax.broadcasted_iota(jnp.int32, (tokens, tokens), 0)
        < lax.broadcasted_iota(jnp.int32, (tokens, tokens), 1),
        1.0,
        0.0,
    ).astype(BF)
    before = jnp.dot((first + second).astype(BF), earlier, preferred_element_type=F32)
    place = before + expert_row.astype(F32) * slots_per
    slot_a = jnp.sum(first * place, axis=0, keepdims=True).astype(jnp.int32)
    slot_b = jnp.sum(second * place, axis=0, keepdims=True).astype(jnp.int32)
    slot_row = lax.broadcasted_iota(jnp.int32, (slots, tokens), 0)
    pick_a = jnp.where(slot_row == slot_a, 1.0, 0.0).astype(BF)
    pick_b = jnp.where(slot_row == slot_b, 1.0, 0.0).astype(BF)
    sent = jnp.dot(pick_a + pick_b, x_ref[...], preferred_element_type=F32).astype(BF)
    x_out[...] = sent.reshape(x_out.shape)
    x_buf[tp, me] = x_out[me]

    pl.semaphore_wait(barrier, n_ep - 1 + n_y)

    def disp(peer):
        return pltpu.make_async_remote_copy(
            x_out.at[peer], x_buf.at[tp, me], di_s.at[peer], di_r.at[me],
            device_id=(peer, tp), device_id_type=MESH,
        )

    def disp_in(source):
        return pltpu.make_async_remote_copy(
            x_out.at[source], x_buf.at[tp, source], di_s.at[source], di_r.at[source],
            device_id=(source, tp), device_id_type=MESH,
        )

    def kv_copy(peer, origin):
        return pltpu.make_async_remote_copy(
            kv_buf.at[origin], kv_buf.at[origin], kv_s.at[peer], kv_r.at[origin],
            device_id=(peer, tp), device_id_type=MESH,
        )

    def over_y(j, source, owner):
        return pltpu.make_async_remote_copy(
            x_buf.at[owner * 2 + core, source], x_buf.at[owner * 2 + core, source],
            dy_s.at[y_peer(j), source], dy_r.at[owner, source],
            device_id=(me, y_peer(j) * 2 + core), device_id_type=MESH,
        )

    def start_disp(o, carry):
        disp((me + o) % n_ep).start()
        return carry

    lax.fori_loop(1, n_ep, start_disp, 0)
    for j in range(1, n_y):
        over_y(j, me, my_y).start()

    own = kv_ref[...].astype(F32)
    turned = prep(own, kg_ref[...], cos_ref[...], sin_ref[...])
    lane = lax.broadcasted_iota(jnp.int32, own.shape, 1)
    kv_buf[me] = jnp.where(lane < HD, turned, own).astype(BF)

    def start_kv(o, carry):
        kv_copy((me + o) % n_ep, me).start()
        return carry

    lax.fori_loop(1, n_ep, start_kv, 0)

    for tile in range(q_ref.shape[1] // LANES):
        q_tile = prep(
            q_ref[:, tile * LANES:(tile + 1) * LANES].astype(F32),
            qg_ref[...], cos_ref[...], sin_ref[...],
        )
        q_lane = lax.broadcasted_iota(jnp.int32, q_tile.shape, 1)
        for part in range(2):
            head = tile * 2 + part
            if head < heads:
                moved = q_tile if part == 0 else pltpu.roll(q_tile, HD, 1)
                q_buf[head] = jnp.where(q_lane < HD, moved, 0.0).astype(BF)

    def forward(o, carry):
        source = (me + n_ep - o) % n_ep
        disp_in(source).wait_recv()
        for j in range(1, n_y):
            over_y(j, source, my_y).start()
        return carry

    lax.fori_loop(1, n_ep, forward, 0)

    def to_mate(owner, mine):
        quarter = owner * 2 + mine
        return pltpu.make_async_remote_copy(
            x_buf.at[quarter], x_buf.at[quarter], dc_s.at[owner], dc_r.at[owner],
            device_id=(me, mate), device_id_type=MESH,
        )

    to_mate(my_y, core).start()
    for j in range(1, n_y):
        owner = y_peer(j)

        def arrived(source, carry):
            over_y(j, source, owner).wait_recv()
            return carry

        lax.fori_loop(0, n_ep, arrived, 0)
        to_mate(owner, core).start()
    for j in range(n_y):
        to_mate(y_peer(j), 1 - core).wait_recv()

    power = jnp.zeros((slots, 1), F32)
    for q in range(n_tp):
        x_q = x_buf[q].reshape(slots, col_w).astype(F32)
        power = power + jnp.sum(x_q * x_q, axis=1, keepdims=True)
        scaled[:, q * col_w:(q + 1) * col_w] = (
            x_q * gain_ref[:, q * col_w:(q + 1) * col_w]
        ).astype(BF)
    row_scale = lax.rsqrt(power * (1.0 / model_width) + EPSILON)
    loads[0].wait()
    loads[1].wait()
    hidden_w = wg.shape[1]
    tile_w = math.gcd(hidden_w, 256)

    def hidden_tile(i, carry):
        cols = pl.ds(pl.multiple_of(i * tile_w, tile_w), tile_w)
        gate = row_scale * jnp.dot(scaled[...], wg[:, cols], preferred_element_type=F32)
        up = row_scale * jnp.dot(scaled[...], wu[:, cols], preferred_element_type=F32)
        hid[:, cols] = (gate / (1.0 + jnp.exp(-gate)) * up).astype(BF)
        return carry

    lax.fori_loop(0, hidden_w // tile_w, hidden_tile, 0)
    loads[2].wait()
    for q in range(n_tp):
        dp_buf[q] = jnp.dot(
            hid[...], wd[:, q * col_w:(q + 1) * col_w], preferred_element_type=F32
        ).astype(BF)

    def expert_mate(owner, side):
        return pltpu.make_async_remote_copy(
            dp_buf.at[owner * 2 + side], ep_in.at[owner], ep_s.at[owner], ep_r.at[owner],
            device_id=(me, mate), device_id_type=MESH,
        )

    def expert_y(j):
        return pltpu.make_async_remote_copy(
            es_buf.at[y_peer(j)], ey_in.at[my_y], ey_s.at[y_peer(j)], ey_r.at[my_y],
            device_id=(me, y_peer(j) * 2 + core), device_id_type=MESH,
        )

    def expert_y_in(j):
        return pltpu.make_async_remote_copy(
            es_buf.at[y_peer(j)], ey_in.at[y_peer(j)], ey_s.at[y_peer(j)], ey_r.at[y_peer(j)],
            device_id=(me, y_peer(j) * 2 + core), device_id_type=MESH,
        )

    for j in range(n_y):
        expert_mate(y_peer((j + 1) % n_y), 1 - core).start()

    def kv_wait(o, carry):
        source = (me + n_ep - o) % n_ep
        kv_copy(source, source).wait_recv()
        return carry

    lax.fori_loop(1, n_ep, kv_wait, 0)

    def mate_sum(j):
        owner = y_peer(j)
        expert_mate(owner, core).wait_recv()
        return dp_buf[owner * 2 + core].astype(F32) + ep_in[owner].astype(F32)

    for j in range(1, n_y):
        es_buf[y_peer(j)] = mate_sum(j).astype(BF)
        expert_y(j).start()

    def ret(peer, origin):
        return pltpu.make_async_remote_copy(
            ret_out.at[peer], ret_in.at[origin], rt_s.at[peer], rt_r.at[origin],
            device_id=(peer, tp), device_id_type=MESH,
        )

    def return_rows():
        total = mate_sum(0)
        for j in range(1, n_y):
            expert_y_in(j).wait_recv()
            total = total + ey_in[y_peer(j)].astype(F32)
        ret_out[...] = total.astype(BF).reshape(ret_out.shape)
        ret_in[me] = ret_out[me]

        def start_ret(o, carry):
            ret((me + o) % n_ep, me).start()
            return carry

        lax.fori_loop(1, n_ep, start_ret, 0)

    piece = rows // n_y
    half = piece // 2
    factor = HD ** (-0.5) * math.log2(math.e)

    def mix_mate(owner, side):
        return pltpu.make_async_remote_copy(
            mp_out.at[owner, side], mp_in.at[owner], mp_s.at[owner], mp_r.at[owner],
            device_id=(me, mate), device_id_type=MESH,
        )

    def mix_y(j, origin):
        return pltpu.make_async_remote_copy(
            ms_out.at[y_peer(j)], my_in.at[origin], my_s.at[y_peer(j)], my_r.at[origin],
            device_id=(me, y_peer(j) * 2 + core), device_id_type=MESH,
        )

    def attend(owner):
        start = pl.multiple_of(owner * piece, piece)
        q_rows = q_buf[:, pl.ds(start, piece), :].reshape(heads * piece, LANES)

        def one_block(block, total):
            kv = kv_buf[block]
            logits = lax.dot_general(
                q_rows, kv, (((1,), (1,)), ((), ())), preferred_element_type=F32
            )
            weights = jnp.exp2(logits * factor).astype(BF)
            kv_lane = lax.broadcasted_iota(jnp.int32, kv.shape, 1)
            values = jnp.where(kv_lane < HD, jnp.ones_like(kv), kv)
            return total + jnp.dot(weights, values, preferred_element_type=F32)

        total = lax.fori_loop(0, n_ep, one_block, jnp.zeros((heads * piece, LANES), F32))
        ratio = (total / pltpu.roll(total, HD, 1)).reshape(heads, piece, LANES)
        out_lane = lax.broadcasted_iota(jnp.int32, (piece, LANES), 1)
        tiles = []
        for tile in range(q_ref.shape[1] // LANES):
            left = pltpu.roll(ratio[2 * tile], HD, 1)
            right = ratio[2 * tile + 1] if 2 * tile + 1 < heads else jnp.zeros_like(left)
            tiles.append(jnp.where(out_lane < HD, left, right).astype(BF))
        attended = tiles[0] if len(tiles) == 1 else jnp.concatenate(tiles, axis=1)
        part = jnp.dot(attended, wmix[...], preferred_element_type=F32).astype(BF)
        mp_out[owner] = part.reshape(2, half, part.shape[1])
        mix_mate(owner, 1 - core).start()

    def mix_sum(owner):
        mix_mate(owner, core).wait_recv()
        return mp_out[owner, core].astype(F32) + mp_in[owner].astype(F32)

    loads[3].wait()
    for j in range(1, n_y):
        attend(y_peer(j))
        if j == 1:
            return_rows()
        ms_out[y_peer(j)] = mix_sum(y_peer(j)).astype(BF)
        mix_y(j, my_y).start()
    attend(my_y)

    def ret_wait(o, carry):
        source = (me + n_ep - o) % n_ep
        ret(source, source).wait_recv()
        return carry

    lax.fori_loop(1, n_ep, ret_wait, 0)
    back = ret_in[...].reshape(slots, col_w)
    share = scores_ref[...] / jnp.sum(scores_ref[...], axis=1, keepdims=True)
    rows_a = lax.dot_general(
        pick_a, back, (((0,), (0,)), ((), ())), preferred_element_type=F32
    )
    rows_b = lax.dot_general(
        pick_b, back, (((0,), (0,)), ((), ())), preferred_element_type=F32
    )
    out_ref[...] = (rows_a * share[:, 0:1] + rows_b * share[:, 1:2]).astype(BF)

    total = mix_sum(my_y)
    for j in range(1, n_y):
        mix_y(j, y_peer(j)).wait_recv()
        total = total + my_in[y_peer(j)].astype(F32)
    mixed_ref[...] = total.astype(BF)

    def sends(o, carry):
        peer = (me + o) % n_ep
        disp(peer).wait_send()
        kv_copy(peer, me).wait_send()
        ret(peer, me).wait_send()
        return carry

    lax.fori_loop(1, n_ep, sends, 0)
    for j in range(1, n_y):

        def sent_y(source, carry):
            over_y(j, source, my_y).wait_send()
            return carry

        lax.fori_loop(0, n_ep, sent_y, 0)
        expert_y(j).wait_send()
        mix_y(j, my_y).wait_send()
    for j in range(n_y):
        to_mate(y_peer(j), core).wait_send()
        expert_mate(y_peer(j), 1 - core).wait_send()
        mix_mate(y_peer(j), 1 - core).wait_send()


def local(
    n_ep, n_tp,
    queries, key_input, value_input, query_gain, key_gain, mix_out_weight, expert_input, ffn_gain,
    routes, route_scores, gate_weight, up_weight, down_weight,
):
    rows = queries.shape[0]
    heads = queries.shape[1] // HD
    tp = lax.axis_index("tp")
    n_y = n_tp // 2
    kv_head = tp * heads // (HEADS // KV_HEADS)
    kv = jnp.concatenate(
        [lax.dynamic_slice_in_dim(a, kv_head * HD, HD, 1) for a in (key_input, value_input)], axis=1
    )
    spare = heads % 2 * HD
    if spare:
        queries = jnp.pad(queries, ((0, 0), (0, spare)))
        mix_out_weight = jnp.pad(mix_out_weight, ((0, spare), (0, 0)))
    positions = lax.axis_index("ep") * rows + jnp.arange(rows, dtype=jnp.int32)
    quarter = HD // 4
    lane = jnp.arange(LANES, dtype=jnp.int32)
    inverse = jnp.tile(ROPE_BASE ** (-jnp.arange(quarter, dtype=F32) / quarter), LANES // quarter)
    place = jnp.where(
        (lane % HD < HD // 2)[None, :], (positions // GRID_W)[:, None], (positions % GRID_W)[:, None]
    ).astype(F32)
    angle = place * inverse[None, :]
    cos_table = jnp.cos(angle)
    sin_table = jnp.sin(angle) * jnp.where(lane % (2 * quarter) < quarter, -1.0, 1.0)[None, :]
    width = expert_input.shape[1]
    col_w = width // n_tp
    tokens, top = routes.shape
    own_x = lax.dynamic_slice_in_dim(expert_input, tp * col_w, col_w, 1)
    capacity = 3 * tokens * top // (2 * n_ep)
    slots_per = -(-capacity // 16) * 16
    slots = n_ep * slots_per
    hidden_w = gate_weight.shape[2]
    out_w = mix_out_weight.shape[1]
    half = rows // n_tp
    vm = pltpu.VMEM
    dma = pltpu.SemaphoreType.DMA
    scratch = [
        vm((n_ep, rows, LANES), BF), vm((heads, rows, LANES), BF),
        vm((n_ep, slots_per, col_w), BF), vm((n_tp, n_ep, slots_per, col_w), BF),
        vm((slots, width), BF), vm((slots, hidden_w), BF),
        vm((width, hidden_w), BF), vm((width, hidden_w), BF), vm((hidden_w, width), BF),
        vm(mix_out_weight.shape, BF),
        vm((n_tp, slots, col_w), BF), vm((n_y, slots, col_w), BF), vm((n_y, slots, col_w), BF),
        vm((n_y, slots, col_w), BF),
        vm((n_ep, slots_per, col_w), BF), vm((n_ep, slots_per, col_w), BF),
        vm((n_y, 2, half, out_w), BF), vm((n_y, half, out_w), BF), vm((n_y, half, out_w), BF),
        vm((n_y, half, out_w), BF), vm((8, LANES), F32),
        dma((4,)),
        dma((n_ep,)), dma((n_ep,)), dma((n_ep,)), dma((n_ep,)),
        dma((n_y, n_ep)), dma((n_y, n_ep)),
    ] + [dma((n_y,))] * 6 + [dma((n_ep,))] * 2 + [dma((n_y,))] * 4
    in_vmem = pl.BlockSpec(memory_space=pltpu.VMEM)
    in_any = pl.BlockSpec(memory_space=pl.ANY)
    return pl.pallas_call(
        functools.partial(kernel, n_ep, n_tp, heads, width),
        out_shape=(
            jax.ShapeDtypeStruct((half, out_w), BF),
            jax.ShapeDtypeStruct((tokens, col_w), BF),
        ),
        in_specs=[in_vmem] * 6 + [in_any] + [in_vmem] * 4 + [in_any] * 3,
        out_specs=(in_vmem, in_vmem),
        scratch_shapes=scratch,
        compiler_params=pltpu.CompilerParams(
            collective_id=0, has_side_effects=True, vmem_limit_bytes=60 * 1024 * 1024
        ),
    )(
        queries, kv,
        jnp.tile(query_gain, LANES // HD)[None, :], jnp.tile(key_gain, LANES // HD)[None, :],
        cos_table, sin_table, mix_out_weight, own_x, ffn_gain[None, :], routes.T, route_scores,
        gate_weight, up_weight, down_weight,
    )


def solution(mesh):
    placed = (
        P("ep", "tp"),
        P("ep", None),
        P("ep", None),
        P(),
        P(),
        P("tp", None),
        P("ep", None),
        P(),
        P("ep", None),
        P("ep", None),
        P("ep", None, "tp"),
        P("ep", None, "tp"),
        P("ep", "tp", None),
    )
    return jax.shard_map(
        functools.partial(local, mesh.shape["ep"], mesh.shape["tp"]),
        mesh=mesh,
        in_specs=placed,
        out_specs=(P(("ep", "tp"), None), P("ep", "tp")),
        check_vma=False,
    )
```

time: 201 us -> 83.9 us (0.42)
  Pallas kernels: 0 us -> 70.1 us
  blocking collectives: 68.3 us -> 0 us
  matrix products: 60.7 us -> 0 us
  waiting for transfers between devices: 19 us -> 0 us
  between operations: 14.2 us -> 0.7 us
  starting transfers between devices: 12.5 us -> 0 us
  other arithmetic: 8.75 us -> 2.62 us
  local copies, waits for them, and re-layouts: 15.4 us -> 9.4 us
    pallas_call x0 -> x1, Pallas kernels: none -> 70.1 us  [local(): pl.pallas_call(functools.partial(kernel, n_ep, n_tp, heads, width), out_s...]
    all_gather x2 -> x0, blocking collectives: 68.3 us -> none  [the longest x1 35.1 us: local(): key_piece = lax.all_gather(own_keys, 'ep', axis=0, tiled=True)]
    dot_general x11 -> x0, matrix products: 60.7 us -> none  [the longest x4 21.6 us: one_block(): jnp.einsum('qgrd,kgd->qgrk', q_rot, key_block, preferred_element_type=jnp...]
    all_to_all x2 -> x0, starting transfers between devices: 12.2 us -> none  [the longest x1 6.25 us: local(): lax.all_to_all(outbound, 'ep', split_axis=0, concat_axis=0, tiled=True)]
    reduce_scatter x2 -> x0, waiting for transfers between devices: 10.7 us -> none  [the longest x1 10.7 us: local(): lax.psum_scatter(jnp.dot(attended, mix_out_weight, preferred_element_type...]
    all_to_all x2 -> x0, waiting for transfers between devices: 8.28 us -> none  [the longest x1 8.28 us: local(): lax.all_to_all(width_sum, 'ep', split_axis=1, concat_axis=1, tiled=True)]
    gather x2 -> x0, local copies, waits for them, and re-layouts: 4.15 us -> none  [the longest x1 2.13 us: local(): outbound = padded[owner_row]]
    all_to_all x4 -> x0, local copies, waits for them, and re-layouts: 3.79 us -> none  [the longest x2 2.01 us: local(): lax.all_to_all(width_sum, 'ep', split_axis=1, concat_axis=1, tiled=True)]
  transfers between devices with their start and end apart: 5 -> 0, of which waited for: 2 -> 0; matrix products, arithmetic and copies ran while one was open for 27% -> 0% of each run, Pallas kernels for 0% -> 0%
where the time goes in v1:
time: 83.9 us; the launch traced here: 82.8 us
  Pallas kernels  70.1 us (84%)
  local copies, waits for them, and re-layouts  9.4 us (11%)
  other arithmetic  2.62 us (3%)
    pallas_call x1, Pallas kernels, local(): pl.pallas_call(functools.partial(kernel, n_ep, n_tp, heads, width), out_s...  70.1 us
    unnamed x5, local copies, waits for them, and re-layouts  4.91 us
    mul x1, other arithmetic, local(): jnp.sin(angle)  1.82 us

profile of v1, /device:TPU:8, one launch (start us, length us, event | category | flops | bytes accessed | tf_op | source)
XLA Modules:
  0.0 82.8 jit_solution(14220052940044603536)
XLA Ops:
  0.6 0.0 copy-start
  0.7 0.7 tile.6
  1.4 0.6 broadcast_in_dim_tile.7.qg_ref
  2.0 0.7 tile.7
  2.7 0.7 broadcast_in_dim_tile.8.kg_ref
  3.3 0.1 mul.34
  3.4 1.4 %copy.15.scores_ref = f32[160,2]{1,0:T(8,128)} copy(f32[160,2]{0,1:T(2,128)} %param.22) | data formatting | bytes 2560 | tf_op args[9]
  4.9 0.0 copy-done
  4.9 0.7 constant_dynamic-slice_fusion.x_ref
  5.5 1.1 %constant_dynamic-slice_fusion.1 = (bf16[512,64]{1,0:T(8,128)(2,1)S(1)}, bf16[512,64]{1,0:T(8,128)(2,1)S(1)}) fusion(bf16[512,256]{1,0:T(8,128)(2,1)} %param.15, s32[]{:T(128)S(6)} %select_n.62, bf16[512,256]{1,0:T(8,128)(2,1)} %param.14), kind=kLoop, calls=%fused_computation.18 | loop fusion | bytes 262148 | tf_op jit(solution)/shard_map/dynamic_slice | solution.py:394
  6.7 0.8 pad_maximum_fusion.kv_ref
  7.4 1.8 %sine_multiply_fusion = (f32[512,128]{1,0:T(8,128)}, f32[512,128]{1,0:T(8,128)}) fusion(f32[128]{0:T(128)S(1)} %compare_select_fusion, f32[128]{0:T(128)S(1)} %mul.34, s32[512]{0:T(512)S(1)} %get-tuple-element.6, s32[512]{0:T(512)S(1)} %get-tuple-element.7, pred[128]{0:T(512)(128)(4,1)S(1)} %fusion.4), kind=kLoop, calls=%fused_computation | loop fusion | flops 262144 | bytes 529536 | tf_op jit(solution)/shard_map/mul | solution.py:409
  9.2 70.1 %shard_map.140 = (bf16[128,2048]{1,0:T(8,128)(2,1)}, bf16[160,512]{1,0:T(8,128)(2,1)}) custom-call(bf16[512,256]{1,0:T(8,128)(2,1)} %q_ref.1, bf16[512,128]{1,0:T(8,128)(2,1)} %pad_maximum_fusion.kv_ref, f32[1,128]{1,0:T(1,128)} %broadcast_in_dim_tile.7.qg_ref, f32[1,128]{1,0:T(1,128)} %broadcast_in_dim_tile.8.kg_ref, f32[512,128]{1,0:T(8,128)} %get-tuple-element.3.cos_ref, ...), custom_call_target="tpu_custom_call" | custom-call | tf_op jit(solution)/shard_map/pallas_call | solution.py:439
  79.3 1.9 %copy.18 = bf16[128,2048]{1,0:T(8,128)(2,1)} copy(bf16[128,2048]{1,0:T(8,128)(2,1)} %get-tuple-element.10) | data formatting | bytes 1048576
  81.2 1.6 %copy.19 = bf16[160,512]{1,0:T(8,128)(2,1)} copy(bf16[160,512]{1,0:T(8,128)(2,1)} %get-tuple-element.11) | data formatting | bytes 327680
  (5 shorter events, 0.0 us)
Async XLA Ops:
  0.6 4.2 %copy-start = (bf16[160,2048]{1,0:T(8,128)(2,1)S(1)}, bf16[160,2048]{1,0:T(8,128)(2,1)}, u32[]{:S(2)}) copy-start(bf16[160,2048]{1,0:T(8,128)(2,1)} %param.19) | copy-start | bytes 1966084

commit v2 on v1

--- a/solution.py
+++ b/solution.py
@@ -31,6 +31,7 @@
     total = jnp.dot(high, same, preferred_element_type=F32) + jnp.dot(
         low, same, preferred_element_type=F32
     )
+    gain = jnp.concatenate([gain] * (width // HD), axis=1)
     normed = values * lax.rsqrt(total * (1.0 / HD) + EPSILON) * gain
     lane = lax.broadcasted_iota(jnp.int32, normed.shape, 1)
     quarter = HD // 4
@@ -42,13 +43,41 @@
     return normed * cos_table + partner * sin_table
 
 
+def angle_tables(start, rows):
+    quarter = HD // 4
+    many = rows // GRID_W
+
+    def both(count, first):
+        shape = (count, LANES)
+        place = lax.broadcasted_iota(jnp.int32, shape, 0) + first
+        lane = lax.broadcasted_iota(jnp.int32, shape, 1)
+        turn = lane % quarter
+        inverse = jnp.zeros(shape, F32)
+        for j in range(quarter):
+            inverse = jnp.where(turn == j, ROPE_BASE ** (-j / quarter), inverse)
+        angle = place.astype(F32) * inverse
+        sign = jnp.where(lane % (2 * quarter) < quarter, -1.0, 1.0)
+        return jnp.cos(angle), jnp.sin(angle) * sign
+
+    tables = []
+    for by_row, by_col in zip(both(max(many, 8), start // GRID_W), both(GRID_W, 0)):
+        lane = lax.broadcasted_iota(jnp.int32, by_col.shape, 1)
+        tables.append(
+            jnp.concatenate(
+                [jnp.where(lane % HD < HD // 2, by_row[i:i + 1, :], by_col) for i in range(many)],
+                axis=0,
+            )
+        )
+    return tables
+
+
 def kernel(
     n_ep, n_tp, heads, model_width,
-    q_ref, kv_ref, qg_ref, kg_ref, cos_ref, sin_ref, wmix_ref, x_ref, gain_ref, routes_ref,
+    q_any, k_any, v_any, qg_ref, kg_ref, wmix_ref, x_any, gain_ref, routes_ref,
     scores_ref, wg_ref, wu_ref, wd_ref,
     mixed_ref, out_ref,
-    kv_buf, q_buf, x_out, x_buf, scaled, hid, wg, wu, wd, wmix, dp_buf, ep_in, es_buf, ey_in,
-    ret_out, ret_in, mp_out, mp_in, ms_out, my_in, own_mix,
+    q_ref, k_in, v_in, x_ref, kv_buf, q_buf, x_out, x_buf, scaled, hid, wg, wu, wd, wmix, dp_buf, ep_in, es_buf, ey_in,
+    ret_out, ret_in, mp_out, mp_in, ms_out, my_in,
     w_sem, kv_s, kv_r, di_s, di_r, dy_s, dy_r, dc_s, dc_r, ep_s, ep_r, ey_s, ey_r, rt_s, rt_r,
     mp_s, mp_r, my_s, my_r,
 ):
@@ -57,11 +86,14 @@
     tp = lax.axis_index("tp")
     my_y, core = tp // 2, tp % 2
     mate = my_y * 2 + 1 - core
-    rows = kv_ref.shape[0]
+    rows = q_ref.shape[0]
+    kv_head = tp * heads // (HEADS // KV_HEADS)
+    kv_tile = pl.ds(pl.multiple_of(kv_head // 2 * LANES, LANES), LANES)
     slots_per = x_buf.shape[2]
     slots = n_ep * slots_per
     col_w = x_buf.shape[3]
     tokens = x_ref.shape[0]
+    x_cols = pl.ds(pl.multiple_of(tp * col_w, col_w), col_w)
 
     def y_peer(j):
         return (my_y + j) % n_y
@@ -69,7 +101,16 @@
     loads = [
         pltpu.make_async_copy(src, dst, w_sem.at[i])
         for i, (src, dst) in enumerate(
-            ((wg_ref.at[0], wg), (wu_ref.at[0], wu), (wd_ref.at[0], wd), (wmix_ref, wmix))
+            (
+                (x_any.at[:, x_cols], x_ref),
+                (k_any.at[:, kv_tile], k_in),
+                (v_any.at[:, kv_tile], v_in),
+                (q_any, q_ref),
+                (wg_ref.at[0], wg),
+                (wu_ref.at[0], wu),
+                (wd_ref.at[0], wd),
+                (wmix_ref, wmix),
+            )
         )
     ]
     for load in loads:
@@ -104,6 +145,7 @@
     slot_row = lax.broadcasted_iota(jnp.int32, (slots, tokens), 0)
     pick_a = jnp.where(slot_row == slot_a, 1.0, 0.0).astype(BF)
     pick_b = jnp.where(slot_row == slot_b, 1.0, 0.0).astype(BF)
+    loads[0].wait()
     sent = jnp.dot(pick_a + pick_b, x_ref[...], preferred_element_type=F32).astype(BF)
     x_out[...] = sent.reshape(x_out.shape)
     x_buf[tp, me] = x_out[me]
@@ -122,9 +164,19 @@
             device_id=(source, tp), device_id_type=MESH,
         )
 
-    def kv_copy(peer, origin):
-        return pltpu.make_async_remote_copy(
-            kv_buf.at[origin], kv_buf.at[origin], kv_s.at[peer], kv_r.at[origin],
+    n_x = 1 << ((n_ep.bit_length() - 1) // 2)
+    n_z = n_ep // n_x
+    my_z, my_x = me // n_x, me % n_x
+
+    def z_peer(o):
+        return (my_z + o) % n_z * n_x + my_x
+
+    def x_peer(o):
+        return my_z * n_x + (my_x + o) % n_x
+
+    def kv_copy(peer, origin, leg):
+        return pltpu.make_async_remote_copy(
+            kv_buf.at[origin], kv_buf.at[origin], kv_s.at[leg], kv_r.at[origin],
             device_id=(peer, tp), device_id_type=MESH,
         )
 
@@ -143,21 +195,23 @@
     for j in range(1, n_y):
         over_y(j, me, my_y).start()
 
-    own = kv_ref[...].astype(F32)
-    turned = prep(own, kg_ref[...], cos_ref[...], sin_ref[...])
-    lane = lax.broadcasted_iota(jnp.int32, own.shape, 1)
-    kv_buf[me] = jnp.where(lane < HD, turned, own).astype(BF)
-
-    def start_kv(o, carry):
-        kv_copy((me + o) % n_ep, me).start()
-        return carry
-
-    lax.fori_loop(1, n_ep, start_kv, 0)
-
+    cos_table, sin_table = angle_tables(me * rows, rows)
+    loads[1].wait()
+    loads[2].wait()
+    odd = kv_head % 2 == 1
+    key = k_in[...].astype(F32)
+    value = v_in[...].astype(F32)
+    key = jnp.where(odd, pltpu.roll(key, HD, 1), key)
+    value = jnp.where(odd, value, pltpu.roll(value, HD, 1))
+    turned = prep(key, kg_ref[...], cos_table, sin_table)
+    lane = lax.broadcasted_iota(jnp.int32, key.shape, 1)
+    kv_buf[me] = jnp.where(lane < HD, turned, value).astype(BF)
+
+    loads[3].wait()
     for tile in range(q_ref.shape[1] // LANES):
         q_tile = prep(
             q_ref[:, tile * LANES:(tile + 1) * LANES].astype(F32),
-            qg_ref[...], cos_ref[...], sin_ref[...],
+            qg_ref[...], cos_table, sin_table,
         )
         q_lane = lax.broadcasted_iota(jnp.int32, q_tile.shape, 1)
         for part in range(2):
@@ -174,6 +228,10 @@
         return carry
 
     lax.fori_loop(1, n_ep, forward, 0)
+    for o in range(1, n_x):
+        kv_copy(x_peer(o), me, o).start()
+    for o in range(1, n_z):
+        kv_copy(z_peer(o), me, o * n_x).start()
 
     def to_mate(owner, mine):
         quarter = owner * 2 + mine
@@ -203,8 +261,8 @@
             x_q * gain_ref[:, q * col_w:(q + 1) * col_w]
         ).astype(BF)
     row_scale = lax.rsqrt(power * (1.0 / model_width) + EPSILON)
-    loads[0].wait()
-    loads[1].wait()
+    loads[4].wait()
+    loads[5].wait()
     hidden_w = wg.shape[1]
     tile_w = math.gcd(hidden_w, 256)
 
@@ -216,12 +274,18 @@
         return carry
 
     lax.fori_loop(0, hidden_w // tile_w, hidden_tile, 0)
-    loads[2].wait()
+    loads[6].wait()
     for q in range(n_tp):
         dp_buf[q] = jnp.dot(
             hid[...], wd[:, q * col_w:(q + 1) * col_w], preferred_element_type=F32
         ).astype(BF)
 
+    for o in range(1, n_z):
+        origin = z_peer(n_z - o)
+        kv_copy(origin, origin, 0).wait_recv()
+        for i in range(1, n_x):
+            kv_copy(x_peer(i), origin, o * n_x + i).start()
+
     def expert_mate(owner, side):
         return pltpu.make_async_remote_copy(
             dp_buf.at[owner * 2 + side], ep_in.at[owner], ep_s.at[owner], ep_r.at[owner],
@@ -242,13 +306,6 @@
 
     for j in range(n_y):
         expert_mate(y_peer((j + 1) % n_y), 1 - core).start()
-
-    def kv_wait(o, carry):
-        source = (me + n_ep - o) % n_ep
-        kv_copy(source, source).wait_recv()
-        return carry
-
-    lax.fori_loop(1, n_ep, kv_wait, 0)
 
     def mate_sum(j):
         owner = y_peer(j)
@@ -326,7 +383,11 @@
         mix_mate(owner, core).wait_recv()
         return mp_out[owner, core].astype(F32) + mp_in[owner].astype(F32)
 
-    loads[3].wait()
+    for o in range(n_z):
+        for i in range(1, n_x):
+            origin = (my_z + n_z - o) % n_z * n_x + (my_x + n_x - i) % n_x
+            kv_copy(x_peer(i), origin, 0).wait_recv()
+    loads[7].wait()
     for j in range(1, n_y):
         attend(y_peer(j))
         if j == 1:
@@ -342,14 +403,21 @@
 
     lax.fori_loop(1, n_ep, ret_wait, 0)
     back = ret_in[...].reshape(slots, col_w)
-    share = scores_ref[...] / jnp.sum(scores_ref[...], axis=1, keepdims=True)
+    share_row = scores_ref[...] / jnp.sum(scores_ref[...], axis=0, keepdims=True)
+    own_token = lax.broadcasted_iota(jnp.int32, (tokens, tokens), 0) == lax.broadcasted_iota(
+        jnp.int32, (tokens, tokens), 1
+    )
+    share_a, share_b = (
+        jnp.sum(jnp.where(own_token, share_row[i:i + 1, :], 0.0), axis=1, keepdims=True)
+        for i in range(2)
+    )
     rows_a = lax.dot_general(
         pick_a, back, (((0,), (0,)), ((), ())), preferred_element_type=F32
     )
     rows_b = lax.dot_general(
         pick_b, back, (((0,), (0,)), ((), ())), preferred_element_type=F32
     )
-    out_ref[...] = (rows_a * share[:, 0:1] + rows_b * share[:, 1:2]).astype(BF)
+    out_ref[...] = (rows_a * share_a + rows_b * share_b).astype(BF)
 
     total = mix_sum(my_y)
     for j in range(1, n_y):
@@ -360,7 +428,7 @@
     def sends(o, carry):
         peer = (me + o) % n_ep
         disp(peer).wait_send()
-        kv_copy(peer, me).wait_send()
+        kv_copy(peer, me, o).wait_send()
         ret(peer, me).wait_send()
         return carry
 
@@ -387,30 +455,14 @@
 ):
     rows = queries.shape[0]
     heads = queries.shape[1] // HD
-    tp = lax.axis_index("tp")
     n_y = n_tp // 2
-    kv_head = tp * heads // (HEADS // KV_HEADS)
-    kv = jnp.concatenate(
-        [lax.dynamic_slice_in_dim(a, kv_head * HD, HD, 1) for a in (key_input, value_input)], axis=1
-    )
     spare = heads % 2 * HD
     if spare:
         queries = jnp.pad(queries, ((0, 0), (0, spare)))
         mix_out_weight = jnp.pad(mix_out_weight, ((0, spare), (0, 0)))
-    positions = lax.axis_index("ep") * rows + jnp.arange(rows, dtype=jnp.int32)
-    quarter = HD // 4
-    lane = jnp.arange(LANES, dtype=jnp.int32)
-    inverse = jnp.tile(ROPE_BASE ** (-jnp.arange(quarter, dtype=F32) / quarter), LANES // quarter)
-    place = jnp.where(
-        (lane % HD < HD // 2)[None, :], (positions // GRID_W)[:, None], (positions % GRID_W)[:, None]
-    ).astype(F32)
-    angle = place * inverse[None, :]
-    cos_table = jnp.cos(angle)
-    sin_table = jnp.sin(angle) * jnp.where(lane % (2 * quarter) < quarter, -1.0, 1.0)[None, :]
     width = expert_input.shape[1]
     col_w = width // n_tp
     tokens, top = routes.shape
-    own_x = lax.dynamic_slice_in_dim(expert_input, tp * col_w, col_w, 1)
     capacity = 3 * tokens * top // (2 * n_ep)
     slots_per = -(-capacity // 16) * 16
     slots = n_ep * slots_per
@@ -420,6 +472,7 @@
     vm = pltpu.VMEM
     dma = pltpu.SemaphoreType.DMA
     scratch = [
+        vm(queries.shape, BF), vm((rows, LANES), BF), vm((rows, LANES), BF), vm((tokens, col_w), BF),
         vm((n_ep, rows, LANES), BF), vm((heads, rows, LANES), BF),
         vm((n_ep, slots_per, col_w), BF), vm((n_tp, n_ep, slots_per, col_w), BF),
         vm((slots, width), BF), vm((slots, hidden_w), BF),
@@ -429,8 +482,8 @@
         vm((n_y, slots, col_w), BF),
         vm((n_ep, slots_per, col_w), BF), vm((n_ep, slots_per, col_w), BF),
         vm((n_y, 2, half, out_w), BF), vm((n_y, half, out_w), BF), vm((n_y, half, out_w), BF),
-        vm((n_y, half, out_w), BF), vm((8, LANES), F32),
-        dma((4,)),
+        vm((n_y, half, out_w), BF),
+        dma((8,)),
         dma((n_ep,)), dma((n_ep,)), dma((n_ep,)), dma((n_ep,)),
         dma((n_y, n_ep)), dma((n_y, n_ep)),
     ] + [dma((n_y,))] * 6 + [dma((n_ep,))] * 2 + [dma((n_y,))] * 4
@@ -442,16 +495,15 @@
             jax.ShapeDtypeStruct((half, out_w), BF),
             jax.ShapeDtypeStruct((tokens, col_w), BF),
         ),
-        in_specs=[in_vmem] * 6 + [in_any] + [in_vmem] * 4 + [in_any] * 3,
+        in_specs=[in_any] * 3 + [in_vmem] * 2 + [in_any] * 2 + [in_vmem] * 3 + [in_any] * 3,
         out_specs=(in_vmem, in_vmem),
         scratch_shapes=scratch,
         compiler_params=pltpu.CompilerParams(
             collective_id=0, has_side_effects=True, vmem_limit_bytes=60 * 1024 * 1024
         ),
     )(
-        queries, kv,
-        jnp.tile(query_gain, LANES // HD)[None, :], jnp.tile(key_gain, LANES // HD)[None, :],
-        cos_table, sin_table, mix_out_weight, own_x, ffn_gain[None, :], routes.T, route_scores,
+        queries, key_input, value_input, query_gain[None, :], key_gain[None, :],
+        mix_out_weight, expert_input, ffn_gain[None, :], routes.T, route_scores.T,
         gate_weight, up_weight, down_weight,
     )
 

time: 83.9 us -> 70.6 us (0.84); the launches traced: 82.8 us -> 70.4 us
  local copies, waits for them, and re-layouts: 9.4 us -> 3.47 us
  Pallas kernels: 70.1 us -> 66.2 us
  other arithmetic: 2.62 us -> 0 us
    pallas_call x1, Pallas kernels: 70.1 us -> 66.2 us  [local(): pl.pallas_call(functools.partial(kernel, n_ep, n_tp, heads, width), out_s...]
    another operation x5 -> x0, local copies, waits for them, and re-layouts: 2.62 us -> none  [the longest x2 1.32 us: local(): jnp.tile(key_gain, LANES // HD)[None, :]]
    mul x1 -> x0, other arithmetic: 1.82 us -> none  [local(): jnp.sin(angle)]
    dynamic_slice x2 -> x0, local copies, waits for them, and re-layouts: 1.78 us -> none  [the longest x1 1.1 us: local(): lax.dynamic_slice_in_dim(a, kv_head * HD, HD, 1)]
    unnamed x5 -> x2, local copies, waits for them, and re-layouts: 4.91 us -> 3.47 us
where the time goes in v2:
time: 70.6 us; the launch traced here: 70.4 us
  Pallas kernels  66.2 us (94%)
  local copies, waits for them, and re-layouts  3.47 us (5%)
    pallas_call x1, Pallas kernels, local(): pl.pallas_call(functools.partial(kernel, n_ep, n_tp, heads, width), out_s...  66.2 us
    unnamed x2, local copies, waits for them, and re-layouts  3.47 us

profile of v2, /device:TPU:8, one launch (start us, length us, event | category | flops | bytes accessed | tf_op | source)
XLA Modules:
  0.0 70.4 jit_solution(13072696709541873627)
XLA Ops:
  0.6 66.2 %shard_map.140 = (bf16[128,2048]{1,0:T(8,128)(2,1)}, bf16[160,512]{1,0:T(8,128)(2,1)}) custom-call(bf16[512,256]{1,0:T(8,128)(2,1)} %q_any.1, bf16[512,256]{1,0:T(8,128)(2,1)} %k_any.1, bf16[512,256]{1,0:T(8,128)(2,1)} %v_any.1, f32[1,64]{1,0:T(1,128)} %bitcast.8, f32[1,64]{1,0:T(1,128)} %bitcast.9, bf16[256,2048]{1,0:T(8,128)(2,1)} %wmix_ref.1, ...), custom_call_target="tpu_custom_call" | custom-call | tf_op jit(solution)/shard_map/pallas_call | solution.py:492
  66.9 1.9 %copy.17 = bf16[128,2048]{1,0:T(8,128)(2,1)} copy(bf16[128,2048]{1,0:T(8,128)(2,1)} %get-tuple-element.4) | data formatting | bytes 1048576
  68.8 1.6 %copy.18 = bf16[160,512]{1,0:T(8,128)(2,1)} copy(bf16[160,512]{1,0:T(8,128)(2,1)} %get-tuple-element.5) | data formatting | bytes 327680
